TPU v7x, 32 devices: a whole 2x2x4 slice. The times are simulated.
32 devices in a mesh: grp: 2 (over y), sp: 4 (over z), tp: 4 (over x, core).
Axes of the slice: x: 2, y: 2, z: 4, core: 2. Of those that a mesh axis runs over, the one named last changes fastest.
Arguments:
- stream: bfloat16 [6144, 4096], P(('grp', 'sp'), 'tp'), parts along dimension 0, may hold values from -400 to 400
- in_weight: bfloat16 [2, 1024, 4096], P(None, 'sp', 'tp'), may hold values from -0.09375 to 0.09375
- out_weight: bfloat16 [2, 1024, 4096], P(None, 'sp', 'tp'), may hold values from -0.1875 to 0.1875
- group_mix: bfloat16 [2, 4, 256, 256], replicated, may hold values from -0.375 to 0.375
- pool_gain: float32 [2, 1024], replicated, may hold values from 0.1 to 1.9
- norm_gain: float32 [2, 4096], P(None, 'tp'), may hold values from 0.1 to 1.9
- norm_shift: float32 [2, 4096], P(None, 'tp'), may hold values from -3 to 3
Outputs:
- refined: bfloat16 [6144, 4096], P(('grp', 'sp'), 'tp'), parts along dimension 0
There are 2 independent parts, one for each index of `grp`. A program takes and returns all parts, laid end to end along the dimension named above; an argument that names none is the same for every part. Nothing has to cross between parts.
All inputs are finite; a program needn't handle non-finite values.
Results may differ from a plain program's by a relative error of at most 0.015.
Values may be sent and summed in bfloat16 or wider, within the bound.
A program may use at most 64 MiB of HBM per device.

v0:
```python
import functools

import jax
import jax.numpy as jnp
from jax import lax
from jax.experimental import pallas as pl
from jax.experimental.pallas import tpu as pltpu
from jax.sharding import PartitionSpec as P

MESH = pl.DeviceIdType.MESH
EPSILON = 1e-05
F32 = jnp.float32
BF16 = jnp.bfloat16
REACH = 16
PIECES = 2
NT = (((1,), (1,)), ((), ()))


def arrival_orders(n):
    orders = []
    for z in range(n):
        first = 1 if z < n / 2 else -1
        order = [z]
        for d in range(1, n):
            order += [b for b in (z + first * d, z - first * d) if 0 <= b < n]
        orders.append(order)
    return orders


def kernel(cfg, *refs):
    n, tp_n, layers, groups, width, streamed = cfg
    (stream, w_in, w_out, mix, gain, norm_gain, norm_shift, out,
     wg, cur, acc, psend, precv, pown, xsend, xrecv, hbuf, hsend, hrecv, sc, tsend, trecv,
     loc_sem, own_send, f_send, z_recv, y_send, y_recv,
     p_send_s, p_recv_s, x_send_s, x_recv_s, h_send_s, h_recv_s,
     c_send_s, c_recv_s, t_send_s, t_recv_s, out_sem) = refs
    tokens, chans = cur.shape
    half = tokens // 2
    block = 256
    chunks = tokens // block
    d_model = chans * tp_n
    alpha = (2.0 * layers) ** 0.25
    nx = tp_n // 2
    y, z, t = lax.axis_index("grp"), lax.axis_index("sp"), lax.axis_index("tp")
    core, x = lax.rem(t, 2), t // 2
    sib = t + 1 - 2 * core
    orders = arrival_orders(n)
    mine, other = core * half, (1 - core) * half
    mine = pl.multiple_of(mine, half)
    other = pl.multiple_of(other, half)

    def order(s):
        if not streamed:
            return jnp.int32(s)
        b = jnp.int32(0)
        for k in range(n):
            b = jnp.where(z == k, orders[k][s], b)
        return b

    def remote(src, dst, ssem, rsem, device):
        return pltpu.make_async_remote_copy(
            src_ref=src, dst_ref=dst, send_sem=ssem, recv_sem=rsem,
            device_id=device, device_id_type=MESH)

    rows = w_in.shape[1]
    copies = [pltpu.make_async_copy(stream, cur, loc_sem.at[0])]
    for m in range(2 * layers):
        src = (w_in, w_out)[m % 2].at[m // 2]
        if streamed:
            dst = wg.at[m, pl.ds(pl.multiple_of(z * rows, rows), rows)]
        else:
            dst = wg.at[m]
        copies.append(pltpu.make_async_copy(src, dst, loc_sem.at[1 + m]))
    for copy in copies:
        copy.start()

    barrier = pltpu.get_barrier_semaphore()

    def greet(device):
        pl.semaphore_signal(barrier, inc=1, device_id=device, device_id_type=MESH)

    for k in range(1, tp_n):
        greet((y, z, lax.rem(t + k, tp_n)))
    count = jnp.int32(tp_n - 1)
    if streamed:
        greet((1 - y, z, t))
        count = count + 1

        @pl.when(z > 0)
        def _():
            greet((y, z - 1, t))

        @pl.when(z < n - 1)
        def _():
            greet((y, z + 1, t))

        count = count + jnp.where(z > 0, 1, 0) + jnp.where(z < n - 1, 1, 0)
    down = (core == 1) & (z < n - 1)
    up = (core == 0) & (z > 0)

    @pl.when(down)
    def _():
        greet((y, z + 1, sib))

    @pl.when(up)
    def _():
        greet((y, z - 1, sib))

    count = count + jnp.where(down, 1, 0) + jnp.where(up, 1, 0)
    pl.semaphore_wait(barrier, count)

    part = rows // 2
    cut = part // PIECES

    def span(base, q):
        return pl.ds(pl.multiple_of(base + q * cut, cut), cut)

    def own_copy(m, side, q):
        src = (w_in, w_out)[m % 2].at[m // 2, span(y * part, q)]
        dst = wg.at[m, span(z * rows + y * part, q)]
        return remote(src, dst, own_send.at[m, side, q], z_recv.at[m, z, q], (y, z + 2 * side - 1, t))

    def own_side(m, side, when, what):
        @pl.when(when & (z < n - 1 if side else z > 0))
        def _():
            for q in range(PIECES):
                what(own_copy(m, side, q))

    def onward(m, b, q):
        zt = jnp.where(b < z, z + 1, z - 1)
        ref = wg.at[m, span(b * rows + y * part, q)]
        return (zt >= 0) & (zt < n), remote(
            ref, ref, f_send.at[m, b, q], z_recv.at[m, b, q], (y, zt, t))

    def across(m, b, from_y, q):
        ref = wg.at[m, span(b * rows + from_y * part, q)]
        return remote(ref, ref, y_send.at[m, b, q], y_recv.at[m, b, q], (1 - y, z, t))

    events = [(m, s, q) for m in range(2 * layers) for s in range(1, n) for q in range(PIECES)]
    state = [0]

    def forwards_end(k, side):
        steps = [s for s in range(1, n) if (orders[k][s] < k if side else orders[k][s] > k)]
        return max(steps, default=0)

    def advance(m, s, ahead=0):
        if not streamed:
            return
        goal = min((m * (n - 1) + s) * PIECES + ahead, len(events))
        while state[0] < goal:
            em, es, q = events[state[0]]
            state[0] += 1
            b = order(es)
            there, copy = onward(em, b, q)
            copy.wait_recv()
            pl.when(there)(copy.start)
            across(em, b, y, q).start()
            if q == PIECES - 1 and em + 1 < 2 * layers:
                for side in (1, 0):
                    places = [k for k in range(n) if forwards_end(k, side) == es]
                    for k in places:
                        own_side(em + 1, side, z == k, lambda c: c.start())

    def ready(m, s):
        if s == 0:
            copies[1 + m].wait()
        elif streamed:
            for q in range(PIECES):
                across(m, order(s), 1 - y, q).wait_recv()

    def weight(m, s):
        return wg[m, pl.ds(pl.multiple_of(order(s) * block, block), block), :]

    def p_copy(l, s):
        return remote(psend.at[l, s], precv.at[l, s], p_send_s.at[l, s], p_recv_s.at[l, s], (y, z, sib))

    def x_copies(l, s):
        return [remote(xsend.at[l, s], xrecv.at[k - 1, l, s], x_send_s.at[k - 1, l, s],
                       x_recv_s.at[k - 1, l, s], (y, z, lax.rem(x + k, nx) * 2 + core))
                for k in range(1, nx)]

    def h_copy(l, s):
        b = order(s)
        return remote(hsend.at[l, b], hrecv.at[l, b], h_send_s.at[l, b], h_recv_s.at[l, b],
                      (y, z + core, sib))

    def c_copy(l, s, at):
        ref = sc.at[l, s, pl.ds(at, half)]
        return remote(ref, ref, c_send_s.at[l, s], c_recv_s.at[l, s], (y, z, sib))

    def t_copies(l, i):
        return [remote(tsend.at[l, i], trecv.at[k - 1, l, i], t_send_s.at[k - 1, l, i],
                       t_recv_s.at[k - 1, l, i], (y, z, lax.rem(t + k, tp_n)))
                for k in range(1, tp_n)]

    h_out = (core == 0) | (z < n - 1)
    h_in = (core == 1) | (z > 0)

    def project(l, s):
        w = weight(2 * l, s)
        psend[l, s] = lax.dot_general(
            cur[pl.ds(other, half), :], w, NT, preferred_element_type=F32).astype(BF16)
        p_copy(l, s).start()
        pown[s] = lax.dot_general(cur[pl.ds(mine, half), :], w, NT, preferred_element_type=F32)

    def chip_sum(l, s):
        p_copy(l, s).wait_recv()
        total = pown[s] + precv[l, s].astype(F32)
        pown[s] = total
        xsend[l, s] = total.astype(BF16)
        for copy in x_copies(l, s):
            copy.start()

    def finish_hidden(l, s):
        total = pown[s]
        for k, copy in enumerate(x_copies(l, s)):
            copy.wait_recv()
            total = total + xrecv[k, l, s].astype(F32)
        hidden = total.astype(BF16)
        hbuf[s, REACH:, :] = hidden.astype(F32)
        hsend[l, order(s)] = hidden[half - REACH:, :]
        pl.when(h_out)(h_copy(l, s).start)

    def pool(l, s):
        b = order(s)

        @pl.when(h_in)
        def _():
            h_copy(l, s).wait_recv()
            hbuf[s, :REACH, :] = hrecv[l, b].astype(F32)

        @pl.when(jnp.logical_not(h_in))
        def _():
            hbuf[s, :REACH, :] = jnp.zeros((REACH, width), F32)

        ext = hbuf[s]
        run = ext + pltpu.roll(ext, 1, 0)
        for octave in range(1, groups):
            take = jnp.where(b >= octave, 1.0, 0.0).astype(F32)
            run = run + take * pltpu.roll(run, 2**octave, 0)
        reach = jnp.int32(2)
        for octave in range(1, groups):
            reach = jnp.where(b >= octave, 2 ** (octave + 1), reach)
        at = z * tokens + core * half + 1 + lax.broadcasted_iota(jnp.int32, (half, width), 0)
        counts = jnp.minimum(at, reach).astype(F32)
        pooled = (run[REACH:, :] / counts - ext[REACH:, :]).astype(BF16)
        mixed = jnp.dot(pooled, mix[l, b], preferred_element_type=F32)
        sc[l, s, pl.ds(mine, half), :] = (mixed * gain[l:l + 1, pl.ds(pl.multiple_of(b * width, width), width)]).astype(BF16)
        c_copy(l, s, mine).start()

    def expand(l, s):
        c_copy(l, s, other).wait_recv()
        at_m = 2 * l + 1

        def body(i, carry):
            r = pl.ds(pl.multiple_of(i * block, block), block)
            add = jnp.dot(sc[l, s, r, :], weight(at_m, s), preferred_element_type=F32)
            if s == 0:
                acc[r, :] = alpha * cur[r, :].astype(F32) + add
            else:
                acc[r, :] = acc[r, :] + add
            return carry

        if s < groups - 1:
            lax.fori_loop(0, chunks, body, 0)
            return
        for i in range(chunks):
            body(i, 0)
            v = acc[i * block:(i + 1) * block, :]
            lane = lax.broadcasted_iota(jnp.int32, (block, 128), 1)
            row_sum = jnp.sum(v, axis=1, keepdims=True)
            row_squares = jnp.sum(v * v, axis=1, keepdims=True)
            both = jnp.where(lane == 0, row_sum, jnp.where(lane == 1, row_squares, 0.0))
            tsend[l, i] = both.T[:8, :]
            for copy in t_copies(l, i):
                copy.start()

    def norm(l):
        dst = out if l == layers - 1 else cur
        for i in range(chunks):
            stats = tsend[l, i]
            for k, copy in enumerate(t_copies(l, i)):
                copy.wait_recv()
                stats = stats + trecv[k, l, i]
            stats = stats / d_model
            mean = stats[0:1, :]
            var = stats[1:2, :] - mean * mean
            inv = lax.rsqrt(var + EPSILON)
            row = lax.broadcasted_iota(jnp.int32, (128, block), 0)
            cols = jnp.where(row == 0, mean, jnp.where(row == 1, inv, 0.0)).T
            r = slice(i * block, (i + 1) * block)
            v = (acc[r, :] - cols[:, 0:1]) * cols[:, 1:2]
            dst[r, :] = (v * norm_gain[l:l + 1, :] + norm_shift[l:l + 1, :]).astype(BF16)

    if streamed:
        for m in range(2 * layers):
            for side in (1, 0):
                first = (z >= 0) if m == 0 else (z == 0 if side else z == n - 1)
                own_side(m, side, first, lambda c: c.start())
    copies[0].wait()
    last = groups - 1
    for l in range(layers):
        mi, mo = 2 * l, 2 * l + 1
        ready(mi, 0)
        project(l, 0)
        for s in range(1, groups):
            advance(mi, s, 2)
            chip_sum(l, s - 1)
            ready(mi, s)
            project(l, s)
        chip_sum(l, last)
        for s in range(groups):
            finish_hidden(l, s)
        pool(l, 0)
        pool(l, 1)
        advance(mo, 2)
        for s in range(2, groups):
            pool(l, s)
        ready(mo, 0)
        expand(l, 0)
        for s in range(1, groups):
            advance(mo, s, 2)
            ready(mo, s)
            expand(l, s)
        norm(l)

    if streamed:
        for m in range(2 * layers):
            for side in (1, 0):
                own_side(m, side, z >= 0, lambda c: c.wait_send())
            for s in range(1, n):
                b = order(s)
                for q in range(PIECES):
                    there, copy = onward(m, b, q)
                    pl.when(there)(copy.wait_send)
                    across(m, b, y, q).wait_send()
    for l in range(layers):
        for s in range(groups):
            p_copy(l, s).wait_send()
            for copy in x_copies(l, s):
                copy.wait_send()
            pl.when(h_out)(h_copy(l, s).wait_send)
            c_copy(l, s, mine).wait_send()
        for i in range(chunks):
            for copy in t_copies(l, i):
                copy.wait_send()


def per_device(n, grp_n, tp_n, stream, in_weight, out_weight, group_mix, pool_gain, norm_gain, norm_shift):
    layers, groups, width = group_mix.shape[:3]
    tokens, chans = stream.shape
    pool = groups * width
    streamed = n == groups and grp_n == 2
    if not streamed:
        in_weight = lax.all_gather(in_weight, "sp", axis=1, tiled=True)
        out_weight = lax.all_gather(out_weight, "sp", axis=1, tiled=True)
    nx = tp_n // 2
    half = tokens // 2
    chunks = tokens // 256
    ms = 2 * layers
    dma = pltpu.SemaphoreType.DMA
    any_spec = pl.BlockSpec(memory_space=pl.ANY)
    vmem = pl.BlockSpec(memory_space=pltpu.VMEM)
    xs = max(nx - 1, 1)
    return pl.pallas_call(
        functools.partial(kernel, (n, tp_n, layers, groups, width, streamed)),
        out_shape=jax.ShapeDtypeStruct((tokens, chans), BF16),
        in_specs=[any_spec] * 3 + [vmem] * 4,
        out_specs=vmem,
        scratch_shapes=[
            pltpu.VMEM((ms, pool, chans), BF16),
            pltpu.VMEM((tokens, chans), BF16),
            pltpu.VMEM((tokens, chans), F32),
            pltpu.VMEM((layers, groups, half, width), BF16),
            pltpu.VMEM((layers, groups, half, width), BF16),
            pltpu.VMEM((groups, half, width), F32),
            pltpu.VMEM((layers, groups, half, width), BF16),
            pltpu.VMEM((xs, layers, groups, half, width), BF16),
            pltpu.VMEM((groups, REACH + half, width), F32),
            pltpu.VMEM((layers, groups, REACH, width), BF16),
            pltpu.VMEM((layers, groups, REACH, width), BF16),
            pltpu.VMEM((layers, groups, tokens, width), BF16),
            pltpu.VMEM((layers, chunks, 8, 256), F32),
            pltpu.VMEM((tp_n - 1, layers, chunks, 8, 256), F32),
            dma((1 + ms,)),
            dma((ms, 2, PIECES)), dma((ms, groups, PIECES)), dma((ms, groups, PIECES)),
            dma((ms, groups, PIECES)), dma((ms, groups, PIECES)),
            dma((layers, groups)), dma((layers, groups)),
            dma((xs, layers, groups)), dma((xs, layers, groups)),
            dma((layers, groups)), dma((layers, groups)),
            dma((layers, groups)), dma((layers, groups)),
            dma((tp_n - 1, layers, chunks)), dma((tp_n - 1, layers, chunks)),
            dma((1,)),
        ],
        compiler_params=pltpu.CompilerParams(
            collective_id=0, has_side_effects=True, vmem_limit_bytes=56 * 1024 * 1024),
    )(stream, in_weight, out_weight, group_mix,
      pool_gain, norm_gain, norm_shift)


def solution(mesh):
    in_specs = (
        P(("grp", "sp"), "tp"),
        P(None, "sp", "tp"),
        P(None, "sp", "tp"),
        P(),
        P(),
        P(None, "tp"),
        P(None, "tp"),
    )
    out_specs = P(("grp", "sp"), "tp")
    sizes = mesh.shape
    body = functools.partial(per_device, sizes["sp"], sizes["grp"], sizes["tp"])
    return jax.shard_map(
        body, mesh=mesh, in_specs=in_specs, out_specs=out_specs, check_vma=False
    )
```

profile of v0, /device:TPU:0, one launch (start us, length us, event | category | flops | bytes accessed | tf_op | source)
XLA Modules:
  0.0 111.6 jit_solution(12441114969377999901)
XLA Ops:
  0.0 108.9 %shard_map.73 = bf16[768,1024]{1,0:T(8,128)(2,1)} custom-call(bf16[768,1024]{1,0:T(8,128)(2,1)} %refs_0_.1, bf16[2,256,1024]{2,1,0:T(8,128)(2,1)} %refs_1_.1, bf16[2,256,1024]{2,1,0:T(8,128)(2,1)} %refs_2_.1, bf16[2,4,256,256]{3,2,1,0:T(8,128)(2,1)} %refs_3_.1, f32[2,1024]{1,0:T(2,128)} %refs_4_.1, f32[2,1024]{1,0:T(2,128)} %refs_5_.1, f32[2,1024]{1,0:T(2,128)} %refs_6_.1), custom_call_target="tpu_custom_call" | custom-call | tf_op jit(solution)/shard_map/pallas_call | solution.py:365
  108.9 2.7 %copy.9 = bf16[768,1024]{1,0:T(8,128)(2,1)} copy(bf16[768,1024]{1,0:T(8,128)(2,1)} %shard_map.73) | data formatting | bytes 3145728
where the time goes:
time: 112 us
  Pallas kernels  109 us (97%)
  local copies, waits for them, and re-layouts  2.67 us (2%)
    pallas_call x1, Pallas kernels, per_device(): pl.pallas_call(functools.partial(kernel, (n, tp_n, layers, groups, width,...  109 us
    unnamed x1, local copies, waits for them, and re-layouts  2.67 us

commit v1 on v0

v1 whole, which is shorter than its diff:
```python
import functools

import jax
import jax.numpy as jnp
from jax import lax
from jax.experimental import pallas as pl
from jax.experimental.pallas import tpu as pltpu
from jax.sharding import PartitionSpec as P

MESH = pl.DeviceIdType.MESH
EPSILON = 1e-05
F32 = jnp.float32
BF16 = jnp.bfloat16
REACH = 16
PIECES = 4
STEPS = (
    ("project", 0), ("chip_sum", 0), ("project", 1), ("chip_sum", 1), ("project", 2), ("chip_sum",
    2), ("project", 3), ("chip_sum", 3), ("finish_hidden", 0), ("pool", 0), ("finish_hidden", 1),
    ("pool", 1), ("expand", 0), ("finish_hidden", 2), ("pool", 2), ("expand", 1), ("finish_hidden",
    3), ("pool", 3), ("expand", 2), ("expand", 3), ("norm", 0), ("norm", 1),
)
EDGE_TICKS = (4, 6, 7, 9, 11, 13, 15, 17, 17, 17, 17, 17, 18, 19, 19, 19, 22, 22, 23, 27, 29, 30, 30, 32, 32,
    33, 35, 37, 39, 41, 41, 41, 41, 41, 42, 43, 43, 44, 47, 47, 47, 48, 48, 48)
INNER_TICKS = (8, 10, 11, 12, 12, 16, 18, 20, 20, 20, 22, 22, 22, 25, 25, 26, 30, 30, 31, 33, 35, 35, 35, 37,
    37, 38, 38, 40, 40, 40, 41, 41, 45, 45, 46, 48, 48, 48, 48, 48, 48, 48, 48, 48)
INNER_ORDER = (1, 2, 1, 2, 1, 2, 1, 2, 3, 3, 3, 3, 1, 2, 1, 2, 1, 2, 1, 2, 3, 3, 3, 3, 1, 1, 1, 2, 1, 2, 2, 3,
    2, 3, 3, 3, 1, 1, 1, 1, 2, 2, 2, 3, 2, 3, 3, 3)
NT = (((1,), (1,)), ((), ()))


def arrival_orders(n):
    orders = []
    for z in range(n):
        first = 1 if z < n / 2 else -1
        order = [z]
        for d in range(1, n):
            order += [b for b in (z + first * d, z - first * d) if 0 <= b < n]
        orders.append(order)
    return orders


def stream_plan(n, layers):
    ms = 2 * layers
    edge = [(m, s, q) for m in range(ms) for s in range(1, n) for q in range(PIECES)]
    seen = [0] * n
    inner = []
    for s in INNER_ORDER:
        inner.append((seen[s] // PIECES, s, seen[s] % PIECES))
        seen[s] += 1
    return edge, inner


def kernel(cfg, *refs):
    n, tp_n, layers, groups, width, streamed = cfg
    (stream, w_in, w_out, mix_in, gain_in, norm_gain_in, norm_shift_in, out,
     mix, gain, norm_gain, norm_shift, wg, cur, acc, psend, precv, pown, xsend, xrecv, hbuf, sc, tsend, trecv, esend, erecv,
     loc_sem, own_send, rest_send, f_send, z_recv, y_send, y_recv,
     p_send_s, p_recv_s, x_send_s, x_recv_s, halo_s,
     c_send_s, c_recv_s, t_send_s, t_recv_s, e_send_s, e_recv_s) = refs
    tokens, chans = stream.shape
    half = tokens // 2
    halo = layers * REACH
    ahead = halo - REACH
    reach_rows = half + halo
    part_rows = half + ahead
    d_model = chans * tp_n
    alpha = (2.0 * layers) ** 0.25
    nx = tp_n // 2
    y, z, t = lax.axis_index("grp"), lax.axis_index("sp"), lax.axis_index("tp")
    core, x = lax.rem(t, 2), t // 2
    sib = t + 1 - 2 * core
    orders = arrival_orders(n)
    mine, other = core * half, (1 - core) * half
    mine = pl.multiple_of(mine, REACH)
    other = pl.multiple_of(other, REACH)

    def order(s):
        if not streamed:
            return jnp.int32(s)
        b = jnp.int32(0)
        for k in range(n):
            b = jnp.where(z == k, orders[k][s], b)
        return b

    def remote(src, dst, ssem, rsem, device):
        return pltpu.make_async_remote_copy(
            src_ref=src, dst_ref=dst, send_sem=ssem, recv_sem=rsem,
            device_id=device, device_id_type=MESH)

    barrier = pltpu.get_barrier_semaphore()

    def greet(device):
        pl.semaphore_signal(barrier, inc=1, device_id=device, device_id_type=MESH)

    for k in range(1, tp_n):
        greet((y, z, lax.rem(t + k, tp_n)))
    count = jnp.int32(tp_n - 1)
    if streamed:
        greet((1 - y, z, t))
        count = count + 1

    @pl.when(z > 0)
    def _():
        greet((y, z - 1, t))

    @pl.when(z < n - 1)
    def _():
        greet((y, z + 1, t))

    count = count + jnp.where(z > 0, 1, 0) + jnp.where(z < n - 1, 1, 0)
    rows = w_in.shape[1]
    copies = [pltpu.make_async_copy(stream, cur.at[pl.ds(halo, tokens)], loc_sem.at[0])]
    for m in range(2 * layers):
        src = (w_in, w_out)[m % 2].at[m // 2]
        if streamed:
            dst = wg.at[m, pl.ds(pl.multiple_of(z * rows, rows), rows)]
        else:
            dst = wg.at[m]
        copies.append(pltpu.make_async_copy(src, dst, loc_sem.at[1 + m]))
    for at, pair in enumerate(((mix_in, mix), (gain_in, gain), (norm_gain_in, norm_gain), (norm_shift_in, norm_shift))):
        copies.append(pltpu.make_async_copy(*pair, loc_sem.at[1 + 2 * layers + at]))
    for copy in copies:
        copy.start()

    pl.semaphore_wait(barrier, count)

    part = rows // 2
    cut = part // PIECES

    def span(base, q):
        return pl.ds(pl.multiple_of(base + q * cut, cut), cut)

    edge = (z == 0) | (z == n - 1)

    def own_copy(m, side, q):
        src = (w_in, w_out)[m % 2].at[m // 2, span(y * part, q)]
        dst = wg.at[m, span(z * rows + y * part, q)]
        return remote(src, dst, own_send.at[m, side, q], z_recv.at[m, z, q], (y, z + 2 * side - 1, t))

    def rest_copy(m, q):
        src = (w_in, w_out)[m % 2].at[m // 2, span((1 - y) * part, q)]
        dst = wg.at[m, span(z * rows + (1 - y) * part, q)]
        return remote(src, dst, rest_send.at[m, q], y_recv.at[m, z, q],
                      (y, jnp.where(z == 0, 1, n - 2), t))

    def own_start(m, k, side):
        if not 0 <= k + 2 * side - 1 < n:
            return

        @pl.when(z == k)
        def _():
            for q in range(PIECES):
                own_copy(m, side, q).start()
            if m == 0 and side:
                halo_copy().start()
            if k in (0, n - 1):
                for q in range(PIECES):
                    rest_copy(m, q).start()

    def onward(m, b, q):
        zt = jnp.where(b < z, z + 1, z - 1)
        ref = wg.at[m, span(b * rows + y * part, q)]
        return (zt >= 0) & (zt < n), remote(
            ref, ref, f_send.at[m, b, q], z_recv.at[m, b, q], (y, zt, t))

    def whole(b):
        return ((z == 1) & (b == 0)) | ((z == n - 2) & (b == n - 1))

    def across(m, b, from_y, q):
        ref = wg.at[m, span(b * rows + from_y * part, q)]
        return remote(ref, ref, y_send.at[m, b, q], y_recv.at[m, b, q], (1 - y, z, t))

    def by_place(values):
        picked = jnp.int32(values[0])
        for k in range(1, n):
            if values[k] != values[0]:
                picked = jnp.where(z == k, values[k], picked)
        return picked

    edge_events, inner_events = stream_plan(n, layers)
    state = [0, 0]

    def take(e_event, i_event):
        places = [k for k in range(n) if (e_event if k in (0, n - 1) else i_event)]

        def go():
            vals = [(e_event if k in (0, n - 1) else i_event) or e_event or i_event for k in range(n)]
            m = by_place([v[0] for v in vals])
            b = by_place([orders[k][v[1]] for k, v in enumerate(vals)])
            q = by_place([v[2] for v in vals])
            there, copy = onward(m, b, q)
            copy.wait_recv()
            pl.when(there)(copy.start)
            pl.when(jnp.logical_not(whole(b)))(across(m, b, y, q).start)

        if len(places) == n:
            go()
        else:
            pl.when(edge if e_event else jnp.logical_not(edge))(go)
        for k in places:
            m, s, q = e_event if k in (0, n - 1) else i_event
            if q != PIECES - 1 or m + 1 >= 2 * layers:
                continue
            if k in (0, n - 1):
                if s == 1:
                    own_start(m + 1, k, 1 if k == 0 else 0)
            elif s == n - 1:
                own_start(m + 1, k, 0 if k < n / 2 else 1)
            elif s == 2:
                own_start(m + 1, k, 1 if k < n / 2 else 0)

    def tick(e_goal, i_goal):
        if not streamed:
            return
        while state[0] < e_goal or state[1] < i_goal:
            e_event = i_event = None
            if state[0] < e_goal:
                e_event = edge_events[state[0]]
                state[0] += 1
            if state[1] < i_goal:
                i_event = inner_events[state[1]]
                state[1] += 1
            take(e_event, i_event)

    def ready(m, s):
        if s == 0:
            copies[1 + m].wait()
        elif streamed:
            for q in range(PIECES):
                across(m, order(s), 1 - y, q).wait_recv()

    def weight(m, s):
        return wg[m, pl.ds(pl.multiple_of(order(s) * width, width), width), :]

    def p_copy(l, s):
        return remote(psend.at[l, s], precv.at[l, s], p_send_s.at[l, s], p_recv_s.at[l, s], (y, z, sib))

    def x_copies(l, s):
        return [remote(xsend.at[l, s], xrecv.at[k - 1, l, s], x_send_s.at[k - 1, l, s],
                       x_recv_s.at[k - 1, l, s], (y, z, lax.rem(x + k, nx) * 2 + core))
                for k in range(1, nx)]

    def halo_copy():
        return remote(stream.at[pl.ds(tokens - halo, halo)], cur.at[pl.ds(0, halo)],
                      halo_s.at[0], halo_s.at[1], (y, jnp.minimum(z + 1, n - 1), t))

    def c_copy(l, s, side):
        ref = sc.at[l, s, side]
        return remote(ref, ref, c_send_s.at[l, s], c_recv_s.at[l, s], (y, z, sib))

    def t_copies(l, i):
        return [remote(tsend.at[l, i], trecv.at[k - 1, l, i], t_send_s.at[k - 1, l, i],
                       t_recv_s.at[k - 1, l, i], (y, z, lax.rem(t + k, tp_n)))
                for k in range(1, tp_n)]

    def e_copies(l):
        return [remote(esend.at[l], erecv.at[k - 1, l], e_send_s.at[k - 1, l],
                       e_recv_s.at[k - 1, l], (y, z, lax.rem(t + k, tp_n)))
                for k in range(1, tp_n)]

    def project(l, s):
        w = weight(2 * l, s)
        psend[l, s] = lax.dot_general(
            cur[pl.ds(other, reach_rows), :], w, NT, preferred_element_type=F32).astype(BF16)
        p_copy(l, s).start()
        pown[s] = lax.dot_general(cur[pl.ds(mine, reach_rows), :], w, NT, preferred_element_type=F32)

    def chip_sum(l, s):
        p_copy(l, s).wait_recv()
        total = pown[s] + precv[l, s].astype(F32)
        pown[s] = total
        xsend[l, s] = total.astype(BF16)
        for copy in x_copies(l, s):
            copy.start()

    def finish_hidden(l, s):
        total = pown[s]
        for k, copy in enumerate(x_copies(l, s)):
            copy.wait_recv()
            total = total + xrecv[k, l, s].astype(F32)
        hbuf[s] = total.astype(BF16).astype(F32)

        @pl.when((z == 0) & (core == 0))
        def _():
            hbuf[s, :halo, :] = jnp.zeros((halo, width), F32)

    def pool(l, s):
        b = order(s)
        ext = hbuf[s]
        run = ext + pltpu.roll(ext, 1, 0)
        for octave in range(1, groups):
            take = jnp.where(b >= octave, 1.0, 0.0).astype(F32)
            run = run + take * pltpu.roll(run, 2**octave, 0)
        reach = jnp.int32(2)
        for octave in range(1, groups):
            reach = jnp.where(b >= octave, 2 ** (octave + 1), reach)
        at = z * tokens + core * half - ahead + 1 + lax.broadcasted_iota(jnp.int32, (part_rows, width), 0)
        counts = jnp.clip(at, 1, reach).astype(F32)
        pooled = (run[REACH:, :] / counts - ext[REACH:, :]).astype(BF16)
        mixed = jnp.dot(pooled, mix[l, b], preferred_element_type=F32)
        sc[l, s, core] = (mixed * gain[l:l + 1, pl.ds(pl.multiple_of(b * width, width), width)]).astype(BF16)
        c_copy(l, s, core).start()

    def grow(l, s, add, rows_at, cur_at):
        if s == 0:
            acc[rows_at, :] = alpha * cur[cur_at, :].astype(F32) + add
        else:
            acc[rows_at, :] = acc[rows_at, :] + add

    def row_totals(v):
        lane = lax.broadcasted_iota(jnp.int32, (v.shape[0], 128), 1)
        row_sum = jnp.sum(v, axis=1, keepdims=True)
        row_squares = jnp.sum(v * v, axis=1, keepdims=True)
        return jnp.where(lane == 0, row_sum, jnp.where(lane == 1, row_squares, 0.0))

    def expand(l, s):
        c_copy(l, s, 1 - core).wait_recv()
        at_m = 2 * l + 1
        extra = l * REACH

        if extra < ahead:
            add = jnp.dot(sc[l, s, 0, extra:ahead, :], weight(at_m, s), preferred_element_type=F32)
            grow(l, s, add, slice(extra, ahead), slice(extra + REACH, halo))
            if s == groups - 1:
                esend[l, extra:, :] = row_totals(acc[extra:ahead, :])
                for copy in e_copies(l):
                    copy.start()

        def body(i, carry):
            add = jnp.dot(sc[l, s, i, ahead:, :], weight(at_m, s), preferred_element_type=F32)
            at = i * half
            if not isinstance(i, int):
                at = pl.multiple_of(at, REACH)
            grow(l, s, add, pl.ds(ahead + at, half), pl.ds(halo + at, half))
            return carry

        if s < groups - 1:
            lax.fori_loop(0, 2, body, 0)
            return
        for i in range(2):
            body(i, 0)
            both = row_totals(acc[ahead + i * half:ahead + (i + 1) * half, :])
            tsend[l, i] = both.T[:8, :]
            for copy in t_copies(l, i):
                copy.start()

    def norm(l, i):
        dst, base = (out, 0) if l == layers - 1 else (cur, halo)
        extra = l * REACH

        def apply(at, mean, inv, size):
            v = (acc[at:at + size, :] - mean) * inv
            to = at - ahead + base
            dst[to:to + size, :] = (v * norm_gain[l:l + 1, :] + norm_shift[l:l + 1, :]).astype(BF16)

        if extra < ahead and i == 0:
            stats = esend[l, extra:, :]
            for k, copy in enumerate(e_copies(l)):
                copy.wait_recv()
                stats = stats + erecv[k, l, extra:, :]
            stats = stats / d_model
            mean = stats[:, 0:1]
            inv = lax.rsqrt(stats[:, 1:2] - mean * mean + EPSILON)
            apply(extra, mean, inv, ahead - extra)
        stats = tsend[l, i]
        for k, copy in enumerate(t_copies(l, i)):
            copy.wait_recv()
            stats = stats + trecv[k, l, i]
        stats = stats / d_model
        mean = stats[0:1, :]
        var = stats[1:2, :] - mean * mean
        inv = lax.rsqrt(var + EPSILON)
        row = lax.broadcasted_iota(jnp.int32, (128, half), 0)
        cols = jnp.where(row == 0, mean, jnp.where(row == 1, inv, 0.0)).T
        apply(ahead + i * half, cols[:, 0:1], cols[:, 1:2], half)

    if streamed:
        for k in range(n):
            for side in (1, 0):
                own_start(0, k, side)
    else:
        pl.when(z < n - 1)(halo_copy().start)

    def before_first():
        @pl.when(z > 0)
        def _():
            halo_copy().wait_recv()

        @pl.when(z == 0)
        def _():
            cur[:halo, :] = jnp.zeros((halo, chans), BF16)

        copies[0].wait()
        for copy in copies[1 + 2 * layers:]:
            copy.wait()

    phases = {"project": project, "chip_sum": chip_sum, "finish_hidden": finish_hidden,
              "pool": pool, "expand": expand, "norm": norm}
    at = 0
    for l in range(layers):
        for name, s in STEPS:
            if at < len(EDGE_TICKS):
                tick(EDGE_TICKS[at], INNER_TICKS[at])
            if at == 0:
                before_first()
            if name == "project":
                ready(2 * l, s)
            elif name == "expand":
                ready(2 * l + 1, s)
            phases[name](l, s)
            at += 1

    if streamed:
        for m in range(2 * layers):
            for side in (1, 0):
                @pl.when((z < n - 1) if side else (z > 0))
                def _():
                    for q in range(PIECES):
                        own_copy(m, side, q).wait_send()

            @pl.when(edge)
            def _():
                for q in range(PIECES):
                    rest_copy(m, q).wait_send()

            for s in range(1, n):
                b = order(s)
                for q in range(PIECES):
                    there, copy = onward(m, b, q)
                    pl.when(there)(copy.wait_send)
                    pl.when(jnp.logical_not(whole(b)))(across(m, b, y, q).wait_send)
    for l in range(layers):
        for s in range(groups):
            p_copy(l, s).wait_send()
            for copy in x_copies(l, s):
                copy.wait_send()
            c_copy(l, s, core).wait_send()
        for i in range(2):
            for copy in t_copies(l, i):
                copy.wait_send()
        if l * REACH < ahead:
            for copy in e_copies(l):
                copy.wait_send()
    pl.when(z < n - 1)(halo_copy().wait_send)


def per_device(n, grp_n, tp_n, stream, in_weight, out_weight, group_mix, pool_gain, norm_gain, norm_shift):
    layers, groups, width = group_mix.shape[:3]
    tokens, chans = stream.shape
    pool = groups * width
    streamed = n == groups == 4 and grp_n == 2 and layers == 2
    if not streamed:
        in_weight = lax.all_gather(in_weight, "sp", axis=1, tiled=True)
        out_weight = lax.all_gather(out_weight, "sp", axis=1, tiled=True)
    nx = tp_n // 2
    half = tokens // 2
    halo = layers * REACH
    ahead = halo - REACH
    ms = 2 * layers
    dma = pltpu.SemaphoreType.DMA
    any_spec = pl.BlockSpec(memory_space=pl.ANY)
    vmem = pl.BlockSpec(memory_space=pltpu.VMEM)
    xs = max(nx - 1, 1)
    return pl.pallas_call(
        functools.partial(kernel, (n, tp_n, layers, groups, width, streamed)),
        out_shape=jax.ShapeDtypeStruct((tokens, chans), BF16),
        in_specs=[any_spec] * 7,
        out_specs=vmem,
        scratch_shapes=[
            pltpu.VMEM(group_mix.shape, BF16),
            pltpu.VMEM(pool_gain.shape, F32),
            pltpu.VMEM(norm_gain.shape, F32),
            pltpu.VMEM(norm_shift.shape, F32),
            pltpu.VMEM((ms, pool, chans), BF16),
            pltpu.VMEM((halo + tokens, chans), BF16),
            pltpu.VMEM((ahead + tokens, chans), F32),
            pltpu.VMEM((layers, groups, halo + half, width), BF16),
            pltpu.VMEM((layers, groups, halo + half, width), BF16),
            pltpu.VMEM((groups, halo + half, width), F32),
            pltpu.VMEM((layers, groups, halo + half, width), BF16),
            pltpu.VMEM((xs, layers, groups, halo + half, width), BF16),
            pltpu.VMEM((groups, halo + half, width), F32),
            pltpu.VMEM((layers, groups, 2, ahead + half, width), BF16),
            pltpu.VMEM((layers, 2, 8, half), F32),
            pltpu.VMEM((tp_n - 1, layers, 2, 8, half), F32),
            pltpu.VMEM((layers, ahead, 128), F32),
            pltpu.VMEM((tp_n - 1, layers, ahead, 128), F32),
            dma((5 + ms,)),
            dma((ms, 2, PIECES)), dma((ms, PIECES)), dma((ms, groups, PIECES)), dma((ms, groups, PIECES)),
            dma((ms, groups, PIECES)), dma((ms, groups, PIECES)),
            dma((layers, groups)), dma((layers, groups)),
            dma((xs, layers, groups)), dma((xs, layers, groups)),
            dma((2,)),
            dma((layers, groups)), dma((layers, groups)),
            dma((tp_n - 1, layers, 2)), dma((tp_n - 1, layers, 2)),
            dma((tp_n - 1, layers)), dma((tp_n - 1, layers)),
        ],
        compiler_params=pltpu.CompilerParams(
            collective_id=0, has_side_effects=True, vmem_limit_bytes=56 * 1024 * 1024),
    )(stream, in_weight, out_weight, group_mix,
      pool_gain, norm_gain, norm_shift)


def solution(mesh):
    in_specs = (
        P(("grp", "sp"), "tp"),
        P(None, "sp", "tp"),
        P(None, "sp", "tp"),
        P(),
        P(),
        P(None, "tp"),
        P(None, "tp"),
    )
    out_specs = P(("grp", "sp"), "tp")
    sizes = mesh.shape
    body = functools.partial(per_device, sizes["sp"], sizes["grp"], sizes["tp"])
    return jax.shard_map(
        body, mesh=mesh, in_specs=in_specs, out_specs=out_specs, check_vma=False
    )
```

time: 112 us -> 90.5 us (0.81)
  Pallas kernels: 109 us -> 87.6 us
    pallas_call x1, Pallas kernels: 109 us -> 87.6 us  [per_device(): pl.pallas_call(functools.partial(kernel, (n, tp_n, layers, groups, width,...]
where the time goes in v1:
time: 90.5 us; the launch traced here: 90.3 us
  Pallas kernels  87.6 us (97%)
  local copies, waits for them, and re-layouts  2.67 us (3%)
    pallas_call x1, Pallas kernels, per_device(): pl.pallas_call(functools.partial(kernel, (n, tp_n, layers, groups, width,...  87.6 us
    unnamed x1, local copies, waits for them, and re-layouts  2.67 us

profile of v1, /device:TPU:0, one launch (start us, length us, event | category | flops | bytes accessed | tf_op | source)
XLA Modules:
  0.0 90.3 jit_solution(14658263109714768725)
XLA Ops:
  0.0 87.6 %shard_map.73 = bf16[768,1024]{1,0:T(8,128)(2,1)} custom-call(bf16[768,1024]{1,0:T(8,128)(2,1)} %refs_0_.1, bf16[2,256,1024]{2,1,0:T(8,128)(2,1)} %refs_1_.1, bf16[2,256,1024]{2,1,0:T(8,128)(2,1)} %refs_2_.1, bf16[2,4,256,256]{3,2,1,0:T(8,128)(2,1)} %refs_3_.1, f32[2,1024]{1,0:T(2,128)} %refs_4_.1, f32[2,1024]{1,0:T(2,128)} %refs_5_.1, f32[2,1024]{1,0:T(2,128)} %refs_6_.1), custom_call_target="tpu_custom_call" | custom-call | tf_op jit(solution)/shard_map/pallas_call | solution.py:464
  87.6 2.7 %copy.9 = bf16[768,1024]{1,0:T(8,128)(2,1)} copy(bf16[768,1024]{1,0:T(8,128)(2,1)} %shard_map.73) | data formatting | bytes 3145728

commit v2 on v1

--- a/solution.py
+++ b/solution.py
@@ -50,13 +50,44 @@
     return edge, inner
 
 
+def mean_and_scale(stats):
+    mean = stats[0:1, :]
+    inv = lax.rsqrt(stats[1:2, :] - mean * mean + EPSILON)
+    row = lax.broadcasted_iota(jnp.int32, (128, stats.shape[1]), 0)
+    cols = jnp.where(row == 0, mean, jnp.where(row == 1, inv, 0.0)).T
+    return cols[:, 0:1], cols[:, 1:2]
+
+
+def finish(d_model, last, summed, totals_in, gain_in, shift_in, out,
+           held, ready, totals, norm_gain, norm_shift, in_sem, out_sem, side_sem):
+    tokens = held.shape[0]
+    size = 256 if tokens % 256 == 0 else 128
+    blocks = [pl.ds(i * size, size) for i in range(tokens // size)]
+    loads = [pltpu.make_async_copy(summed.at[r], held.at[r], in_sem.at[i]) for i, r in enumerate(blocks)]
+    stores = [pltpu.make_async_copy(ready.at[r], out.at[r], out_sem.at[i]) for i, r in enumerate(blocks)]
+    sides = [pltpu.make_async_copy(a, b, side_sem.at[i]) for i, (a, b) in enumerate(
+        ((totals_in, totals), (gain_in, norm_gain), (shift_in, norm_shift)))]
+    for load in sides + loads:
+        load.start()
+    for side in sides:
+        side.wait()
+    for i, r in enumerate(blocks):
+        mean, inv = mean_and_scale(totals[:, i * size:(i + 1) * size] / d_model)
+        loads[i].wait()
+        v = (held[r, :] - mean) * inv
+        ready[r, :] = (v * norm_gain[last:last + 1, :] + norm_shift[last:last + 1, :]).astype(BF16)
+        stores[i].start()
+    for store in stores:
+        store.wait()
+
+
 def kernel(cfg, *refs):
     n, tp_n, layers, groups, width, streamed = cfg
-    (stream, w_in, w_out, mix_in, gain_in, norm_gain_in, norm_shift_in, out,
+    (stream, w_in, w_out, mix_in, gain_in, norm_gain_in, norm_shift_in, out, totals_out,
      mix, gain, norm_gain, norm_shift, wg, cur, acc, psend, precv, pown, xsend, xrecv, hbuf, sc, tsend, trecv, esend, erecv,
-     loc_sem, own_send, rest_send, f_send, z_recv, y_send, y_recv,
+     loc_sem, stream_send, z_recv, y_recv,
      p_send_s, p_recv_s, x_send_s, x_recv_s, halo_s,
-     c_send_s, c_recv_s, t_send_s, t_recv_s, e_send_s, e_recv_s) = refs
+     c_send_s, c_recv_s, t_send_s, t_recv_s, e_send_s, e_recv_s, out_sem) = refs
     tokens, chans = stream.shape
     half = tokens // 2
     halo = layers * REACH
@@ -132,15 +163,19 @@
 
     edge = (z == 0) | (z == n - 1)
 
+    def place(b, zt):
+        return b - jnp.where(b > zt, 1, 0)
+
     def own_copy(m, side, q):
         src = (w_in, w_out)[m % 2].at[m // 2, span(y * part, q)]
         dst = wg.at[m, span(z * rows + y * part, q)]
-        return remote(src, dst, own_send.at[m, side, q], z_recv.at[m, z, q], (y, z + 2 * side - 1, t))
+        zt = z + 2 * side - 1
+        return remote(src, dst, stream_send.at[0], z_recv.at[m, place(z, zt), q], (y, zt, t))
 
     def rest_copy(m, q):
         src = (w_in, w_out)[m % 2].at[m // 2, span((1 - y) * part, q)]
         dst = wg.at[m, span(z * rows + (1 - y) * part, q)]
-        return remote(src, dst, rest_send.at[m, q], y_recv.at[m, z, q],
+        return remote(src, dst, stream_send.at[0], y_recv.at[m, z],
                       (y, jnp.where(z == 0, 1, n - 2), t))
 
     def own_start(m, k, side):
@@ -157,18 +192,22 @@
                 for q in range(PIECES):
                     rest_copy(m, q).start()
 
+    def arrived(m, b, q):
+        ref = wg.at[m, span(b * rows + y * part, q)]
+        remote(ref, ref, stream_send.at[0], z_recv.at[m, place(b, z), q], (y, z, t)).wait_recv()
+
     def onward(m, b, q):
         zt = jnp.where(b < z, z + 1, z - 1)
         ref = wg.at[m, span(b * rows + y * part, q)]
         return (zt >= 0) & (zt < n), remote(
-            ref, ref, f_send.at[m, b, q], z_recv.at[m, b, q], (y, zt, t))
+            ref, ref, stream_send.at[0], z_recv.at[m, place(b, zt), q], (y, zt, t))
 
     def whole(b):
         return ((z == 1) & (b == 0)) | ((z == n - 2) & (b == n - 1))
 
     def across(m, b, from_y, q):
         ref = wg.at[m, span(b * rows + from_y * part, q)]
-        return remote(ref, ref, y_send.at[m, b, q], y_recv.at[m, b, q], (1 - y, z, t))
+        return remote(ref, ref, stream_send.at[0], y_recv.at[m, b], (1 - y, z, t))
 
     def by_place(values):
         picked = jnp.int32(values[0])
@@ -189,7 +228,7 @@
             b = by_place([orders[k][v[1]] for k, v in enumerate(vals)])
             q = by_place([v[2] for v in vals])
             there, copy = onward(m, b, q)
-            copy.wait_recv()
+            arrived(m, b, q)
             pl.when(there)(copy.start)
             pl.when(jnp.logical_not(whole(b)))(across(m, b, y, q).start)
 
@@ -226,17 +265,18 @@
         if s == 0:
             copies[1 + m].wait()
         elif streamed:
-            for q in range(PIECES):
-                across(m, order(s), 1 - y, q).wait_recv()
+            b = order(s)
+            ref = wg.at[m, pl.ds(pl.multiple_of(b * rows + (1 - y) * part, part), part)]
+            remote(ref, ref, stream_send.at[0], y_recv.at[m, b], (y, z, t)).wait_recv()
 
     def weight(m, s):
         return wg[m, pl.ds(pl.multiple_of(order(s) * width, width), width), :]
 
     def p_copy(l, s):
-        return remote(psend.at[l, s], precv.at[l, s], p_send_s.at[l, s], p_recv_s.at[l, s], (y, z, sib))
+        return remote(psend.at[l, s], precv.at[l, s], p_send_s.at[0], p_recv_s.at[l, s], (y, z, sib))
 
     def x_copies(l, s):
-        return [remote(xsend.at[l, s], xrecv.at[k - 1, l, s], x_send_s.at[k - 1, l, s],
+        return [remote(xsend.at[l, s], xrecv.at[k - 1, l, s], x_send_s.at[0],
                        x_recv_s.at[k - 1, l, s], (y, z, lax.rem(x + k, nx) * 2 + core))
                 for k in range(1, nx)]
 
@@ -246,17 +286,20 @@
 
     def c_copy(l, s, side):
         ref = sc.at[l, s, side]
-        return remote(ref, ref, c_send_s.at[l, s], c_recv_s.at[l, s], (y, z, sib))
+        return remote(ref, ref, c_send_s.at[0], c_recv_s.at[l, s], (y, z, sib))
 
     def t_copies(l, i):
-        return [remote(tsend.at[l, i], trecv.at[k - 1, l, i], t_send_s.at[k - 1, l, i],
-                       t_recv_s.at[k - 1, l, i], (y, z, lax.rem(t + k, tp_n)))
+        return [remote(tsend.at[l, i], trecv.at[k - 1, l, i], t_send_s.at[0],
+                       t_recv_s.at[l, i], (y, z, lax.rem(t + k, tp_n)))
                 for k in range(1, tp_n)]
 
     def e_copies(l):
-        return [remote(esend.at[l], erecv.at[k - 1, l], e_send_s.at[k - 1, l],
-                       e_recv_s.at[k - 1, l], (y, z, lax.rem(t + k, tp_n)))
+        return [remote(esend.at[l], erecv.at[k - 1, l], e_send_s.at[0],
+                       e_recv_s.at[l], (y, z, lax.rem(t + k, tp_n)))
                 for k in range(1, tp_n)]
+
+    def settle(ref, sem):
+        pltpu.make_async_copy(ref, ref, sem).wait()
 
     def project(l, s):
         w = weight(2 * l, s)
@@ -343,36 +386,39 @@
             tsend[l, i] = both.T[:8, :]
             for copy in t_copies(l, i):
                 copy.start()
+            if l == layers - 1:
+                out_copy(i).start()
+
+    def out_copy(i):
+        return pltpu.make_async_copy(
+            acc.at[pl.ds(ahead + i * half, half)], out.at[pl.ds(i * half, half)], out_sem.at[i])
 
     def norm(l, i):
-        dst, base = (out, 0) if l == layers - 1 else (cur, halo)
         extra = l * REACH
 
         def apply(at, mean, inv, size):
             v = (acc[at:at + size, :] - mean) * inv
-            to = at - ahead + base
-            dst[to:to + size, :] = (v * norm_gain[l:l + 1, :] + norm_shift[l:l + 1, :]).astype(BF16)
+            to = at - ahead + halo
+            cur[to:to + size, :] = (v * norm_gain[l:l + 1, :] + norm_shift[l:l + 1, :]).astype(BF16)
 
         if extra < ahead and i == 0:
             stats = esend[l, extra:, :]
-            for k, copy in enumerate(e_copies(l)):
-                copy.wait_recv()
+            settle(erecv.at[:, l], e_recv_s.at[l])
+            for k in range(tp_n - 1):
                 stats = stats + erecv[k, l, extra:, :]
             stats = stats / d_model
             mean = stats[:, 0:1]
             inv = lax.rsqrt(stats[:, 1:2] - mean * mean + EPSILON)
             apply(extra, mean, inv, ahead - extra)
         stats = tsend[l, i]
-        for k, copy in enumerate(t_copies(l, i)):
-            copy.wait_recv()
+        settle(trecv.at[:, l, i], t_recv_s.at[l, i])
+        for k in range(tp_n - 1):
             stats = stats + trecv[k, l, i]
-        stats = stats / d_model
-        mean = stats[0:1, :]
-        var = stats[1:2, :] - mean * mean
-        inv = lax.rsqrt(var + EPSILON)
-        row = lax.broadcasted_iota(jnp.int32, (128, half), 0)
-        cols = jnp.where(row == 0, mean, jnp.where(row == 1, inv, 0.0)).T
-        apply(ahead + i * half, cols[:, 0:1], cols[:, 1:2], half)
+        if l == layers - 1:
+            totals_out[:, i * half:(i + 1) * half] = stats
+            return
+        apply(ahead + i * half, *mean_and_scale(stats / d_model), half)
+
 
     if streamed:
         for k in range(n):
@@ -393,6 +439,23 @@
         copies[0].wait()
         for copy in copies[1 + 2 * layers:]:
             copy.wait()
+
+    def drain():
+        if streamed:
+            @pl.when(edge)
+            def _():
+                settle(wg.at[:, pl.ds(0, (n + 1) * part)], stream_send.at[0])
+
+            @pl.when(jnp.logical_not(edge))
+            def _():
+                settle(wg.at[:, pl.ds(0, (2 * n - 1) * part)], stream_send.at[0])
+        settle(psend, p_send_s.at[0])
+        if nx > 1:
+            settle(xrecv, x_send_s.at[0])
+        settle(sc.at[:, :, core], c_send_s.at[0])
+        settle(trecv, t_send_s.at[0])
+        settle(erecv.at[:, pl.ds(0, layers - 1)], e_send_s.at[0])
+        pl.when(z < n - 1)(halo_copy().wait_send)
 
     phases = {"project": project, "chip_sum": chip_sum, "finish_hidden": finish_hidden,
               "pool": pool, "expand": expand, "norm": norm}
@@ -410,38 +473,9 @@
             phases[name](l, s)
             at += 1
 
-    if streamed:
-        for m in range(2 * layers):
-            for side in (1, 0):
-                @pl.when((z < n - 1) if side else (z > 0))
-                def _():
-                    for q in range(PIECES):
-                        own_copy(m, side, q).wait_send()
-
-            @pl.when(edge)
-            def _():
-                for q in range(PIECES):
-                    rest_copy(m, q).wait_send()
-
-            for s in range(1, n):
-                b = order(s)
-                for q in range(PIECES):
-                    there, copy = onward(m, b, q)
-                    pl.when(there)(copy.wait_send)
-                    pl.when(jnp.logical_not(whole(b)))(across(m, b, y, q).wait_send)
-    for l in range(layers):
-        for s in range(groups):
-            p_copy(l, s).wait_send()
-            for copy in x_copies(l, s):
-                copy.wait_send()
-            c_copy(l, s, core).wait_send()
-        for i in range(2):
-            for copy in t_copies(l, i):
-                copy.wait_send()
-        if l * REACH < ahead:
-            for copy in e_copies(l):
-                copy.wait_send()
-    pl.when(z < n - 1)(halo_copy().wait_send)
+    drain()
+    for i in range(2):
+        out_copy(i).wait()
 
 
 def per_device(n, grp_n, tp_n, stream, in_weight, out_weight, group_mix, pool_gain, norm_gain, norm_shift):
@@ -461,11 +495,11 @@
     any_spec = pl.BlockSpec(memory_space=pl.ANY)
     vmem = pl.BlockSpec(memory_space=pltpu.VMEM)
     xs = max(nx - 1, 1)
-    return pl.pallas_call(
+    summed, totals = pl.pallas_call(
         functools.partial(kernel, (n, tp_n, layers, groups, width, streamed)),
-        out_shape=jax.ShapeDtypeStruct((tokens, chans), BF16),
+        out_shape=(jax.ShapeDtypeStruct((tokens, chans), F32), jax.ShapeDtypeStruct((8, tokens), F32)),
         in_specs=[any_spec] * 7,
-        out_specs=vmem,
+        out_specs=(any_spec, vmem),
         scratch_shapes=[
             pltpu.VMEM(group_mix.shape, BF16),
             pltpu.VMEM(pool_gain.shape, F32),
@@ -486,19 +520,36 @@
             pltpu.VMEM((layers, ahead, 128), F32),
             pltpu.VMEM((tp_n - 1, layers, ahead, 128), F32),
             dma((5 + ms,)),
-            dma((ms, 2, PIECES)), dma((ms, PIECES)), dma((ms, groups, PIECES)), dma((ms, groups, PIECES)),
-            dma((ms, groups, PIECES)), dma((ms, groups, PIECES)),
-            dma((layers, groups)), dma((layers, groups)),
-            dma((xs, layers, groups)), dma((xs, layers, groups)),
+            dma((1,)), dma((ms, groups - 1, PIECES)), dma((ms, groups)),
+            dma((1,)), dma((layers, groups)),
+            dma((1,)), dma((xs, layers, groups)),
             dma((2,)),
-            dma((layers, groups)), dma((layers, groups)),
-            dma((tp_n - 1, layers, 2)), dma((tp_n - 1, layers, 2)),
-            dma((tp_n - 1, layers)), dma((tp_n - 1, layers)),
+            dma((1,)), dma((layers, groups)),
+            dma((1,)), dma((layers, 2)),
+            dma((1,)), dma((layers,)),
+            dma((2,)),
         ],
         compiler_params=pltpu.CompilerParams(
             collective_id=0, has_side_effects=True, vmem_limit_bytes=56 * 1024 * 1024),
     )(stream, in_weight, out_weight, group_mix,
       pool_gain, norm_gain, norm_shift)
+    steps = tokens // (256 if tokens % 256 == 0 else 128)
+    return pl.pallas_call(
+        functools.partial(finish, chans * tp_n, layers - 1),
+        out_shape=jax.ShapeDtypeStruct((tokens, chans), BF16),
+        in_specs=[any_spec] * 4,
+        out_specs=any_spec,
+        scratch_shapes=[
+            pltpu.VMEM((tokens, chans), F32),
+            pltpu.VMEM((tokens, chans), BF16),
+            pltpu.VMEM((8, tokens), F32),
+            pltpu.VMEM(norm_gain.shape, F32),
+            pltpu.VMEM(norm_shift.shape, F32),
+            dma((steps,)),
+            dma((steps,)),
+            dma((3,)),
+        ],
+    )(summed, totals, norm_gain, norm_shift)
 
 
 def solution(mesh):

time: 90.5 us -> 87.3 us (0.965)
  local copies, waits for them, and re-layouts: 2.67 us -> 0 us
    pallas_call x1, Pallas kernels: 87.6 us -> 83.8 us  [per_device(): pl.pallas_call(functools.partial(kernel, (n, tp_n, layers, groups, width,...]
    pallas_call x0 -> x1, Pallas kernels: none -> 3.17 us  [per_device(): pl.pallas_call(functools.partial(finish, chans * tp_n, layers - 1), out_s...]
    unnamed x1 -> x0, local copies, waits for them, and re-layouts: 2.67 us -> none
where the time goes in v2:
time: 87.3 us; the launch traced here: 87.1 us
  Pallas kernels  87 us (100%)
    pallas_call x1, Pallas kernels, per_device(): pl.pallas_call(functools.partial(kernel, (n, tp_n, layers, groups, width,...  83.8 us
    pallas_call x1, Pallas kernels, per_device(): pl.pallas_call(functools.partial(finish, chans * tp_n, layers - 1), out_s...  3.17 us

profile of v2, /device:TPU:0, one launch (start us, length us, event | category | flops | bytes accessed | tf_op | source)
XLA Modules:
  0.0 87.1 jit_solution(985530681106835256)
XLA Ops:
  0.0 83.8 %shard_map.73 = (f32[768,1024]{1,0:T(8,128)}, f32[8,768]{1,0:T(8,128)}) custom-call(bf16[768,1024]{1,0:T(8,128)(2,1)} %refs_0_.1, bf16[2,256,1024]{2,1,0:T(8,128)(2,1)} %refs_1_.1, bf16[2,256,1024]{2,1,0:T(8,128)(2,1)} %refs_2_.1, bf16[2,4,256,256]{3,2,1,0:T(8,128)(2,1)} %refs_3_.1, f32[2,1024]{1,0:T(2,128)} %refs_4_.1, f32[2,1024]{1,0:T(2,128)} %gain_in.1, ...), custom_call_target="tpu_custom_call" | custom-call | tf_op jit(solution)/shard_map/pallas_call | solution.py:498
  83.8 3.2 %shard_map.74 = bf16[768,1024]{1,0:T(8,128)(2,1)} custom-call(f32[768,1024]{1,0:T(8,128)} %get-tuple-element.7.summed, f32[8,768]{1,0:T(8,128)} %get-tuple-element.8.totals_in, f32[2,1024]{1,0:T(2,128)} %gain_in.1, f32[2,1024]{1,0:T(2,128)} %shift_in.1), custom_call_target="tpu_custom_call" | custom-call | tf_op jit(solution)/shard_map/pallas_call | solution.py:537

commit v3 on v2

--- a/solution.py
+++ b/solution.py
@@ -13,6 +13,7 @@
 BF16 = jnp.bfloat16
 REACH = 16
 PIECES = 4
+GIFT = 2
 STEPS = (
     ("project", 0), ("chip_sum", 0), ("project", 1), ("chip_sum", 1), ("project", 2), ("chip_sum",
     2), ("project", 3), ("chip_sum", 3), ("finish_hidden", 0), ("pool", 0), ("finish_hidden", 1),
@@ -230,7 +231,8 @@
             there, copy = onward(m, b, q)
             arrived(m, b, q)
             pl.when(there)(copy.start)
-            pl.when(jnp.logical_not(whole(b)))(across(m, b, y, q).start)
+            given = edge & (m == 2 * layers - 1) & (b == n - 1 - z) & (q >= PIECES - GIFT)
+            pl.when(jnp.logical_not(whole(b) | given))(across(m, b, y, q).start)
 
         if len(places) == n:
             go()
@@ -440,15 +442,28 @@
         for copy in copies[1 + 2 * layers:]:
             copy.wait()
 
+    def gift():
+        m = 2 * layers - 1
+        zt = jnp.where(z == 1, 0, n - 1)
+
+        @pl.when(jnp.logical_not(edge))
+        def _():
+            for q in range(PIECES - GIFT, PIECES):
+                b = order(n - 1)
+                ref = wg.at[m, span(b * rows + (1 - y) * part, q)]
+                remote(ref, ref, stream_send.at[0], y_recv.at[m, b], (y, zt, t)).start()
+
     def drain():
         if streamed:
+            given = GIFT * cut // (2 * layers)
+
             @pl.when(edge)
             def _():
-                settle(wg.at[:, pl.ds(0, (n + 1) * part)], stream_send.at[0])
+                settle(wg.at[:, pl.ds(0, (n + 1) * part - given)], stream_send.at[0])
 
             @pl.when(jnp.logical_not(edge))
             def _():
-                settle(wg.at[:, pl.ds(0, (2 * n - 1) * part)], stream_send.at[0])
+                settle(wg.at[:, pl.ds(0, (2 * n - 1) * part + given)], stream_send.at[0])
         settle(psend, p_send_s.at[0])
         if nx > 1:
             settle(xrecv, x_send_s.at[0])
@@ -470,6 +485,8 @@
                 ready(2 * l, s)
             elif name == "expand":
                 ready(2 * l + 1, s)
+                if streamed and l == layers - 1 and s == groups - 1:
+                    gift()
             phases[name](l, s)
             at += 1
 

time: 87.3 us -> 84.9 us (0.973)
  Pallas kernels: 87 us -> 84.5 us
    pallas_call x1, Pallas kernels: 83.8 us -> 81.4 us  [per_device(): pl.pallas_call(functools.partial(kernel, (n, tp_n, layers, groups, width,...]
where the time goes in v3:
time: 84.9 us; the launch traced here: 84.7 us
  Pallas kernels  84.5 us (100%)
    pallas_call x1, Pallas kernels, per_device(): pl.pallas_call(functools.partial(kernel, (n, tp_n, layers, groups, width,...  81.4 us
    pallas_call x1, Pallas kernels, per_device(): pl.pallas_call(functools.partial(finish, chans * tp_n, layers - 1), out_s...  3.17 us

profile of v3, /device:TPU:0, one launch (start us, length us, event | category | flops | bytes accessed | tf_op | source)
XLA Modules:
  0.0 84.7 jit_solution(6400949135148555738)
XLA Ops:
  0.0 81.4 %shard_map.73 = (f32[768,1024]{1,0:T(8,128)}, f32[8,768]{1,0:T(8,128)}) custom-call(bf16[768,1024]{1,0:T(8,128)(2,1)} %refs_0_.1, bf16[2,256,1024]{2,1,0:T(8,128)(2,1)} %refs_1_.1, bf16[2,256,1024]{2,1,0:T(8,128)(2,1)} %refs_2_.1, bf16[2,4,256,256]{3,2,1,0:T(8,128)(2,1)} %refs_3_.1, f32[2,1024]{1,0:T(2,128)} %refs_4_.1, f32[2,1024]{1,0:T(2,128)} %gain_in.1, ...), custom_call_target="tpu_custom_call" | custom-call | tf_op jit(solution)/shard_map/pallas_call | solution.py:515
  81.4 3.2 %shard_map.74 = bf16[768,1024]{1,0:T(8,128)(2,1)} custom-call(f32[768,1024]{1,0:T(8,128)} %get-tuple-element.7.summed, f32[8,768]{1,0:T(8,128)} %get-tuple-element.8.totals_in, f32[2,1024]{1,0:T(2,128)} %gain_in.1, f32[2,1024]{1,0:T(2,128)} %shift_in.1), custom_call_target="tpu_custom_call" | custom-call | tf_op jit(solution)/shard_map/pallas_call | solution.py:554

commit v4 on v3

--- a/solution.py
+++ b/solution.py
@@ -85,8 +85,8 @@
 def kernel(cfg, *refs):
     n, tp_n, layers, groups, width, streamed = cfg
     (stream, w_in, w_out, mix_in, gain_in, norm_gain_in, norm_shift_in, out, totals_out,
-     mix, gain, norm_gain, norm_shift, wg, cur, acc, psend, precv, pown, xsend, xrecv, hbuf, sc, tsend, trecv, esend, erecv,
-     loc_sem, stream_send, z_recv, y_recv,
+     mix, gain, norm_gain, norm_shift, wg, cur, acc, psend, precv, pown, xsend, xrecv, hbuf, sc, held, tsend, trecv, esend, erecv,
+     loc_sem, stream_send, z_recv, y_recv, gift_recv,
      p_send_s, p_recv_s, x_send_s, x_recv_s, halo_s,
      c_send_s, c_recv_s, t_send_s, t_recv_s, e_send_s, e_recv_s, out_sem) = refs
     tokens, chans = stream.shape
@@ -164,18 +164,42 @@
 
     edge = (z == 0) | (z == n - 1)
 
+    side_cols = chans // 2
+    col_cut = side_cols // PIECES
+
+    def by_columns(m):
+        return m == 2 * layers - 1
+
+    def columns(side, q):
+        return pl.ds(pl.multiple_of(side * side_cols + q * col_cut, 128), col_cut)
+
+    def block_rows(b):
+        return pl.ds(pl.multiple_of(b * width, width), width)
+
+    def piece(cols, m, b, side, q):
+        if cols:
+            return wg.at[m, block_rows(b), columns(side, q)]
+        return wg.at[m, span(b * rows + side * part, q)]
+
+    def own_piece(m, side, q):
+        w = (w_in, w_out)[m % 2].at[m // 2]
+        return w.at[:, columns(side, q)] if by_columns(m) else w.at[span(side * part, q)]
+
+    def half_block(m, b, side):
+        if by_columns(m):
+            return wg.at[m, block_rows(b), pl.ds(pl.multiple_of(side * side_cols, 128), side_cols)]
+        return wg.at[m, pl.ds(pl.multiple_of(b * rows + side * part, part), part)]
+
     def place(b, zt):
         return b - jnp.where(b > zt, 1, 0)
 
     def own_copy(m, side, q):
-        src = (w_in, w_out)[m % 2].at[m // 2, span(y * part, q)]
-        dst = wg.at[m, span(z * rows + y * part, q)]
+        src, dst = own_piece(m, y, q), piece(by_columns(m), m, z, y, q)
         zt = z + 2 * side - 1
         return remote(src, dst, stream_send.at[0], z_recv.at[m, place(z, zt), q], (y, zt, t))
 
     def rest_copy(m, q):
-        src = (w_in, w_out)[m % 2].at[m // 2, span((1 - y) * part, q)]
-        dst = wg.at[m, span(z * rows + (1 - y) * part, q)]
+        src, dst = own_piece(m, 1 - y, q), piece(by_columns(m), m, z, 1 - y, q)
         return remote(src, dst, stream_send.at[0], y_recv.at[m, z],
                       (y, jnp.where(z == 0, 1, n - 2), t))
 
@@ -193,21 +217,21 @@
                 for q in range(PIECES):
                     rest_copy(m, q).start()
 
-    def arrived(m, b, q):
-        ref = wg.at[m, span(b * rows + y * part, q)]
+    def arrived(cols, m, b, q):
+        ref = piece(cols, m, b, y, q)
         remote(ref, ref, stream_send.at[0], z_recv.at[m, place(b, z), q], (y, z, t)).wait_recv()
 
-    def onward(m, b, q):
+    def onward(cols, m, b, q):
         zt = jnp.where(b < z, z + 1, z - 1)
-        ref = wg.at[m, span(b * rows + y * part, q)]
+        ref = piece(cols, m, b, y, q)
         return (zt >= 0) & (zt < n), remote(
             ref, ref, stream_send.at[0], z_recv.at[m, place(b, zt), q], (y, zt, t))
 
     def whole(b):
         return ((z == 1) & (b == 0)) | ((z == n - 2) & (b == n - 1))
 
-    def across(m, b, from_y, q):
-        ref = wg.at[m, span(b * rows + from_y * part, q)]
+    def across(cols, m, b, q):
+        ref = piece(cols, m, b, y, q)
         return remote(ref, ref, stream_send.at[0], y_recv.at[m, b], (1 - y, z, t))
 
     def by_place(values):
@@ -223,16 +247,18 @@
     def take(e_event, i_event):
         places = [k for k in range(n) if (e_event if k in (0, n - 1) else i_event)]
 
+        cols = by_columns((e_event or i_event)[0])
+
         def go():
             vals = [(e_event if k in (0, n - 1) else i_event) or e_event or i_event for k in range(n)]
             m = by_place([v[0] for v in vals])
             b = by_place([orders[k][v[1]] for k, v in enumerate(vals)])
             q = by_place([v[2] for v in vals])
-            there, copy = onward(m, b, q)
-            arrived(m, b, q)
+            there, copy = onward(cols, m, b, q)
+            arrived(cols, m, b, q)
             pl.when(there)(copy.start)
             given = edge & (m == 2 * layers - 1) & (b == n - 1 - z) & (q >= PIECES - GIFT)
-            pl.when(jnp.logical_not(whole(b) | given))(across(m, b, y, q).start)
+            pl.when(jnp.logical_not(whole(b) | given))(across(cols, m, b, q).start)
 
         if len(places) == n:
             go()
@@ -261,14 +287,18 @@
             if state[1] < i_goal:
                 i_event = inner_events[state[1]]
                 state[1] += 1
-            take(e_event, i_event)
+            if e_event and i_event and by_columns(e_event[0]) != by_columns(i_event[0]):
+                take(e_event, None)
+                take(None, i_event)
+            else:
+                take(e_event, i_event)
 
     def ready(m, s):
         if s == 0:
             copies[1 + m].wait()
         elif streamed:
             b = order(s)
-            ref = wg.at[m, pl.ds(pl.multiple_of(b * rows + (1 - y) * part, part), part)]
+            ref = half_block(m, b, 1 - y)
             remote(ref, ref, stream_send.at[0], y_recv.at[m, b], (y, z, t)).wait_recv()
 
     def weight(m, s):
@@ -382,14 +412,49 @@
         if s < groups - 1:
             lax.fori_loop(0, 2, body, 0)
             return
+        if l == layers - 1:
+            side = lax.rem(y, 2)
+            early = (PIECES - GIFT) * col_cut
+            widen(l, s, side, 0, side_cols)
+            if streamed:
+                ready_last(at_m, s)
+                gift()
+            widen(l, s, 1 - side, 0, early)
+            if streamed:
+                ready_given(s)
+            widen(l, s, 1 - side, early, side_cols - early)
+            return
         for i in range(2):
             body(i, 0)
             both = row_totals(acc[ahead + i * half:ahead + (i + 1) * half, :])
             tsend[l, i] = both.T[:8, :]
             for copy in t_copies(l, i):
                 copy.start()
-            if l == layers - 1:
-                out_copy(i).start()
+
+    def widen(l, s, side, start, size):
+        final = start > 0
+        at = pl.ds(pl.multiple_of(side * side_cols + start, 128), size)
+        w = wg[2 * l + 1, block_rows(order(s)), at]
+        for i in range(2):
+            r = pl.ds(ahead + i * half, half)
+            v = acc[r, at] + jnp.dot(sc[l, s, i, ahead:, :], w, preferred_element_type=F32)
+            acc[r, at] = v
+            strips = [v[:, k:k + 128] for k in range(0, size, 128)]
+            sums = functools.reduce(jnp.add, strips)
+            squares = functools.reduce(jnp.add, [u * u for u in strips])
+            if size < side_cols:
+                sums, squares = held[0, i] + sums, held[1, i] + squares
+            if not final:
+                held[0, i], held[1, i] = sums, squares
+                continue
+            row_sum = jnp.sum(sums, axis=1, keepdims=True)
+            row_squares = jnp.sum(squares, axis=1, keepdims=True)
+            lane = lax.broadcasted_iota(jnp.int32, (half, 128), 1)
+            both = jnp.where(lane == 0, row_sum, jnp.where(lane == 1, row_squares, 0.0))
+            tsend[l, i] = both.T[:8, :]
+            for copy in t_copies(l, i):
+                copy.start()
+            out_copy(i).start()
 
     def out_copy(i):
         return pltpu.make_async_copy(
@@ -442,16 +507,35 @@
         for copy in copies[1 + 2 * layers:]:
             copy.wait()
 
+    def given_part(b, side):
+        at = side * side_cols + (PIECES - GIFT) * col_cut
+        return wg.at[2 * layers - 1, block_rows(b), pl.ds(pl.multiple_of(at, 128), GIFT * col_cut)]
+
     def gift():
-        m = 2 * layers - 1
         zt = jnp.where(z == 1, 0, n - 1)
 
         @pl.when(jnp.logical_not(edge))
         def _():
-            for q in range(PIECES - GIFT, PIECES):
-                b = order(n - 1)
-                ref = wg.at[m, span(b * rows + (1 - y) * part, q)]
-                remote(ref, ref, stream_send.at[0], y_recv.at[m, b], (y, zt, t)).start()
+            ref = given_part(order(n - 1), 1 - y)
+            remote(ref, ref, stream_send.at[0], gift_recv.at[0], (y, zt, t)).start()
+
+    def ready_last(m, s):
+        b = order(s)
+
+        @pl.when(edge)
+        def _():
+            ref = wg.at[m, block_rows(b), pl.ds(pl.multiple_of((1 - y) * side_cols, 128), (PIECES - GIFT) * col_cut)]
+            remote(ref, ref, stream_send.at[0], y_recv.at[m, b], (y, z, t)).wait_recv()
+
+        @pl.when(jnp.logical_not(edge))
+        def _():
+            ready(m, s)
+
+    def ready_given(s):
+        @pl.when(edge)
+        def _():
+            ref = given_part(order(s), 1 - y)
+            remote(ref, ref, stream_send.at[0], gift_recv.at[0], (y, z, t)).wait_recv()
 
     def drain():
         if streamed:
@@ -483,14 +567,13 @@
                 before_first()
             if name == "project":
                 ready(2 * l, s)
-            elif name == "expand":
+            elif name == "expand" and (l, s) != (layers - 1, groups - 1):
                 ready(2 * l + 1, s)
-                if streamed and l == layers - 1 and s == groups - 1:
-                    gift()
+            if l == layers - 1 and (name, s) == ("norm", 0):
+                drain()
             phases[name](l, s)
             at += 1
 
-    drain()
     for i in range(2):
         out_copy(i).wait()
 
@@ -532,12 +615,13 @@
             pltpu.VMEM((xs, layers, groups, halo + half, width), BF16),
             pltpu.VMEM((groups, halo + half, width), F32),
             pltpu.VMEM((layers, groups, 2, ahead + half, width), BF16),
+            pltpu.VMEM((2, 2, half, 128), F32),
             pltpu.VMEM((layers, 2, 8, half), F32),
             pltpu.VMEM((tp_n - 1, layers, 2, 8, half), F32),
             pltpu.VMEM((layers, ahead, 128), F32),
             pltpu.VMEM((tp_n - 1, layers, ahead, 128), F32),
             dma((5 + ms,)),
-            dma((1,)), dma((ms, groups - 1, PIECES)), dma((ms, groups)),
+            dma((1,)), dma((ms, groups - 1, PIECES)), dma((ms, groups)), dma((1,)),
             dma((1,)), dma((layers, groups)),
             dma((1,)), dma((xs, layers, groups)),
             dma((2,)),

time: 84.9 us -> 84.5 us (level)
  no operation moved by 1% of the time
where the time goes in v4:
time: 84.5 us; the launch traced here: 84.4 us
  Pallas kernels  84.2 us (100%)
    pallas_call x1, Pallas kernels, per_device(): pl.pallas_call(functools.partial(kernel, (n, tp_n, layers, groups, width,...  81 us
    pallas_call x1, Pallas kernels, per_device(): pl.pallas_call(functools.partial(finish, chans * tp_n, layers - 1), out_s...  3.17 us

profile of v4, /device:TPU:0, one launch (start us, length us, event | category | flops | bytes accessed | tf_op | source)
XLA Modules:
  0.0 84.4 jit_solution(7984710812068704074)
XLA Ops:
  0.0 81.0 %shard_map.73 = (f32[768,1024]{1,0:T(8,128)}, f32[8,768]{1,0:T(8,128)}) custom-call(bf16[768,1024]{1,0:T(8,128)(2,1)} %refs_0_.1, bf16[2,256,1024]{2,1,0:T(8,128)(2,1)} %refs_1_.1, bf16[2,256,1024]{2,1,0:T(8,128)(2,1)} %refs_2_.1, bf16[2,4,256,256]{3,2,1,0:T(8,128)(2,1)} %refs_3_.1, f32[2,1024]{1,0:T(2,128)} %refs_4_.1, f32[2,1024]{1,0:T(2,128)} %gain_in.1, ...), custom_call_target="tpu_custom_call" | custom-call | tf_op jit(solution)/shard_map/pallas_call | solution.py:598
  81.0 3.2 %shard_map.74 = bf16[768,1024]{1,0:T(8,128)(2,1)} custom-call(f32[768,1024]{1,0:T(8,128)} %get-tuple-element.7.summed, f32[8,768]{1,0:T(8,128)} %get-tuple-element.8.totals_in, f32[2,1024]{1,0:T(2,128)} %gain_in.1, f32[2,1024]{1,0:T(2,128)} %shift_in.1), custom_call_target="tpu_custom_call" | custom-call | tf_op jit(solution)/shard_map/pallas_call | solution.py:638

commit v5 on v4

--- a/solution.py
+++ b/solution.py
@@ -200,7 +200,7 @@
 
     def rest_copy(m, q):
         src, dst = own_piece(m, 1 - y, q), piece(by_columns(m), m, z, 1 - y, q)
-        return remote(src, dst, stream_send.at[0], y_recv.at[m, z],
+        return remote(src, dst, stream_send.at[0], y_recv.at[m, place(z, jnp.where(z == 0, 1, n - 2))],
                       (y, jnp.where(z == 0, 1, n - 2), t))
 
     def own_start(m, k, side):
@@ -232,7 +232,7 @@
 
     def across(cols, m, b, q):
         ref = piece(cols, m, b, y, q)
-        return remote(ref, ref, stream_send.at[0], y_recv.at[m, b], (1 - y, z, t))
+        return remote(ref, ref, stream_send.at[0], y_recv.at[m, place(b, z)], (1 - y, z, t))
 
     def by_place(values):
         picked = jnp.int32(values[0])
@@ -299,17 +299,17 @@
         elif streamed:
             b = order(s)
             ref = half_block(m, b, 1 - y)
-            remote(ref, ref, stream_send.at[0], y_recv.at[m, b], (y, z, t)).wait_recv()
+            remote(ref, ref, stream_send.at[0], y_recv.at[m, place(b, z)], (y, z, t)).wait_recv()
 
     def weight(m, s):
         return wg[m, pl.ds(pl.multiple_of(order(s) * width, width), width), :]
 
     def p_copy(l, s):
-        return remote(psend.at[l, s], precv.at[l, s], p_send_s.at[0], p_recv_s.at[l, s], (y, z, sib))
+        return remote(psend.at[l, s], precv.at[l, s], p_send_s.at[0], p_recv_s.at[s], (y, z, sib))
 
     def x_copies(l, s):
         return [remote(xsend.at[l, s], xrecv.at[k - 1, l, s], x_send_s.at[0],
-                       x_recv_s.at[k - 1, l, s], (y, z, lax.rem(x + k, nx) * 2 + core))
+                       x_recv_s.at[k - 1, s], (y, z, lax.rem(x + k, nx) * 2 + core))
                 for k in range(1, nx)]
 
     def halo_copy():
@@ -318,7 +318,7 @@
 
     def c_copy(l, s, side):
         ref = sc.at[l, s, side]
-        return remote(ref, ref, c_send_s.at[0], c_recv_s.at[l, s], (y, z, sib))
+        return remote(ref, ref, c_send_s.at[0], c_recv_s.at[s], (y, z, sib))
 
     def t_copies(l, i):
         return [remote(tsend.at[l, i], trecv.at[k - 1, l, i], t_send_s.at[0],
@@ -525,7 +525,7 @@
         @pl.when(edge)
         def _():
             ref = wg.at[m, block_rows(b), pl.ds(pl.multiple_of((1 - y) * side_cols, 128), (PIECES - GIFT) * col_cut)]
-            remote(ref, ref, stream_send.at[0], y_recv.at[m, b], (y, z, t)).wait_recv()
+            remote(ref, ref, stream_send.at[0], y_recv.at[m, place(b, z)], (y, z, t)).wait_recv()
 
         @pl.when(jnp.logical_not(edge))
         def _():
@@ -621,11 +621,11 @@
             pltpu.VMEM((layers, ahead, 128), F32),
             pltpu.VMEM((tp_n - 1, layers, ahead, 128), F32),
             dma((5 + ms,)),
-            dma((1,)), dma((ms, groups - 1, PIECES)), dma((ms, groups)), dma((1,)),
-            dma((1,)), dma((layers, groups)),
-            dma((1,)), dma((xs, layers, groups)),
+            dma((1,)), dma((ms, groups - 1, PIECES)), dma((ms, groups - 1)), dma((1,)),
+            dma((1,)), dma((groups,)),
+            dma((1,)), dma((xs, groups)),
             dma((2,)),
-            dma((1,)), dma((layers, groups)),
+            dma((1,)), dma((groups,)),
             dma((1,)), dma((layers, 2)),
             dma((1,)), dma((layers,)),
             dma((2,)),

time: 84.5 us -> 84.4 us (level)
  no operation moved by 1% of the time
where the time goes in v5:
time: 84.4 us; the launch traced here: 84.2 us
  Pallas kernels  84 us (100%)
    pallas_call x1, Pallas kernels, per_device(): pl.pallas_call(functools.partial(kernel, (n, tp_n, layers, groups, width,...  80.9 us
    pallas_call x1, Pallas kernels, per_device(): pl.pallas_call(functools.partial(finish, chans * tp_n, layers - 1), out_s...  3.17 us

profile of v5, /device:TPU:0, one launch (start us, length us, event | category | flops | bytes accessed | tf_op | source)
XLA Modules:
  0.0 84.2 jit_solution(1183899119795491946)
XLA Ops:
  0.0 80.9 %shard_map.73 = (f32[768,1024]{1,0:T(8,128)}, f32[8,768]{1,0:T(8,128)}) custom-call(bf16[768,1024]{1,0:T(8,128)(2,1)} %refs_0_.1, bf16[2,256,1024]{2,1,0:T(8,128)(2,1)} %refs_1_.1, bf16[2,256,1024]{2,1,0:T(8,128)(2,1)} %refs_2_.1, bf16[2,4,256,256]{3,2,1,0:T(8,128)(2,1)} %refs_3_.1, f32[2,1024]{1,0:T(2,128)} %refs_4_.1, f32[2,1024]{1,0:T(2,128)} %gain_in.1, ...), custom_call_target="tpu_custom_call" | custom-call | tf_op jit(solution)/shard_map/pallas_call | solution.py:598
  80.9 3.2 %shard_map.74 = bf16[768,1024]{1,0:T(8,128)(2,1)} custom-call(f32[768,1024]{1,0:T(8,128)} %get-tuple-element.7.summed, f32[8,768]{1,0:T(8,128)} %get-tuple-element.8.totals_in, f32[2,1024]{1,0:T(2,128)} %gain_in.1, f32[2,1024]{1,0:T(2,128)} %shift_in.1), custom_call_target="tpu_custom_call" | custom-call | tf_op jit(solution)/shard_map/pallas_call | solution.py:638
